TPU v7x, 32 devices: a whole 2x2x4 slice. The times are simulated.
32 devices in a mesh: ep: 8 (over z, x), tp: 4 (over y, core).
Axes of the slice: x: 2, y: 2, z: 4, core: 2. Of those that a mesh axis runs over, the one named last changes fastest.
Arguments:
- out_gate: bfloat16 [4096, 2048], P(('ep', 'tp')), may hold values from -6 to 6
- in_gate: bfloat16 [4096, 2048], P(('ep', 'tp')), may hold values from -6 to 6
- values: bfloat16 [4096, 2048], P(('ep', 'tp')), may hold values from -6 to 6
- conv_taps: float32 [3, 2048], replicated, may hold values from -4 to 4
- out_weight: bfloat16 [2048, 2048], P(None, 'tp'), may hold values from -0.125 to 0.125
- expert_input: bfloat16 [8192, 2048], P(('ep', 'tp')), may hold values from -6 to 6
- norm_gain: float32 [2048], replicated, may hold values from 0.1 to 1.9
- expert_ids: int32 [8192, 2], P(('ep', 'tp')), may hold values from 0 to 7, all different within a row; in each aligned block of 256 rows (0 to 255, 256 to 511, ...) at most 128 rows name the same one
- route_logits: float32 [8192, 2], P(('ep', 'tp')), may hold values from -8 to 8
- group_share: float32 [8192], P(('ep', 'tp')), may hold values from 0.3 to 1
- gate_weight: bfloat16 [8, 2048, 512], P('ep'), may hold values from -0.125 to 0.125
- up_weight: bfloat16 [8, 2048, 512], P('ep'), may hold values from -0.125 to 0.125
- down_weight: bfloat16 [8, 512, 2048], P('ep'), may hold values from -0.25 to 0.25
Outputs:
- mixer_out: bfloat16 [4096, 2048], P(('ep', 'tp'))
- expert_mix: bfloat16 [8192, 2048], P(('ep', 'tp'))
Inputs may be any that keep to these rules, and one draw needn't show every extreme that they name: `expert_ids`: each row names 2 different experts. Within the rows of one device (aligned blocks of 256 rows) no expert is named by more than 128 rows, a bound that some block reaches.
All inputs are finite; a program needn't handle non-finite values.
Results may differ from a plain program's by a relative error of at most 0.0071.
Values may be sent and summed in bfloat16 or wider, within the bound.
No kernel may reach another device: no remote copies, remote signals or barrier semaphores. Data moves between devices by JAX's collectives and lax.ppermute only.
A program may use at most 128 MiB of HBM per device.

v0:
```python
import jax
import jax.numpy as jnp
from jax import lax
from jax.sharding import PartitionSpec as P

SEQS = 1


norm_eps = 1e-05


def passed_along(value, axis, by):
    length = lax.axis_size(axis)
    pairs = [(i, i + by) for i in range(length) if 0 <= i + by < length]
    return lax.ppermute(value, axis, pairs)


def local(
    out_gate,
    in_gate,
    values,
    conv_taps,
    out_weight,
    expert_input,
    norm_gain,
    expert_ids,
    route_logits,
    group_share,
    gate_weight,
    up_weight,
    down_weight,
):
    rows_mix, width = out_gate.shape
    extent = conv_taps.shape[0] - 1
    gated = (in_gate.astype(jnp.float32) * values.astype(jnp.float32)).astype(jnp.bfloat16)
    before = passed_along(gated[rows_mix - extent :], ("ep", "tp"), 1)
    extended = jnp.concatenate([before, gated], axis=0)
    devices = lax.axis_size("ep") * lax.axis_size("tp")
    seq_len = devices * rows_mix // SEQS
    position = lax.axis_index(("ep", "tp")) * rows_mix + jnp.arange(rows_mix, dtype=jnp.int32)
    offset = position % seq_len
    filtered = jnp.zeros((rows_mix, width), jnp.float32)
    for delays in range(extent + 1):
        lagged = extended[extent - delays : extent - delays + rows_mix].astype(jnp.float32)
        if delays > 0:
            lagged = jnp.where((offset >= delays)[:, None], lagged, 0.0)
        filtered = filtered + conv_taps[extent - delays] * lagged
    mixed_rows = (out_gate.astype(jnp.float32) * filtered).astype(jnp.bfloat16)
    mixer_out = jnp.dot(
        mixed_rows,
        lax.all_gather(out_weight, "tp", axis=1, tiled=True),
        preferred_element_type=jnp.float32,
    ).astype(jnp.bfloat16)
    tokens, width = expert_input.shape
    chosen = expert_ids.shape[1]
    experts = lax.axis_size("ep") * gate_weight.shape[0]
    capacity = 2 * tokens * chosen // experts
    inputs = expert_input.astype(jnp.float32)
    scale = lax.rsqrt(jnp.mean(inputs * inputs, axis=-1, keepdims=True) + norm_eps)
    normed = (inputs * scale * norm_gain).astype(jnp.bfloat16)
    flat_ids = expert_ids.reshape(-1)
    entries = flat_ids.shape[0]
    one_hot = (flat_ids[:, None] == jnp.arange(experts, dtype=jnp.int32)[None, :]).astype(jnp.int32)
    earlier = jnp.cumsum(one_hot, axis=0) - one_hot
    slots = jnp.sum(earlier * one_hot, axis=1)
    target = flat_ids * capacity + slots
    owner = (
        jnp.zeros((experts * capacity,), jnp.int32)
        .at[target]
        .set(jnp.arange(entries, dtype=jnp.int32) // chosen)
    )
    filled = jnp.zeros((experts * capacity,), jnp.bfloat16).at[target].set(1.0)
    outgoing = (normed[owner] * filled[:, None]).reshape(experts, capacity, width)
    arrived = lax.all_to_all(outgoing, "ep", split_axis=0, concat_axis=0, tiled=True)
    rows = arrived.reshape(-1, width)
    gate = jnp.dot(rows, gate_weight[0], preferred_element_type=jnp.float32)
    upper = jnp.dot(rows, up_weight[0], preferred_element_type=jnp.float32)
    hidden = (jax.nn.silu(gate) * upper).astype(jnp.bfloat16)
    result = jnp.dot(hidden, down_weight[0], preferred_element_type=jnp.float32).astype(
        jnp.bfloat16
    )
    results = result.reshape(arrived.shape)
    returned = lax.all_to_all(results, "ep", split_axis=0, concat_axis=0, tiled=True)
    picked = returned.reshape(experts * capacity, width)[target].reshape(tokens, chosen, width)
    margin = route_logits[:, 0] - route_logits[:, 1]
    route_weight = group_share[:, None] * jnp.stack(
        [jax.nn.sigmoid(margin), jax.nn.sigmoid(-margin)], axis=1
    )
    expert_mix = jnp.sum(picked.astype(jnp.float32) * route_weight[:, :, None], axis=1).astype(
        jnp.bfloat16
    )
    return (mixer_out, expert_mix)


def solution(mesh):
    return jax.shard_map(
        local,
        mesh=mesh,
        in_specs=(
            P(("ep", "tp"), None),
            P(("ep", "tp"), None),
            P(("ep", "tp"), None),
            P(),
            P(None, "tp"),
            P(("ep", "tp"), None),
            P(),
            P(("ep", "tp"), None),
            P(("ep", "tp"), None),
            P(("ep", "tp")),
            P("ep", None, None),
            P("ep", None, None),
            P("ep", None, None),
        ),
        out_specs=(P(("ep", "tp"), None), P(("ep", "tp"), None)),
        check_vma=False,
    )
```

profile of v0, /device:TPU:0, one launch (start us, length us, event | category | flops | bytes accessed | tf_op | source)
XLA Modules:
  0.0 275.4 jit_solution(744212111417791703)
XLA Ops:
  7.2 1.0 copy.17
  8.4 0.7 broadcast_multiply_fusion.1
  9.1 1.1 reduce-window.6
  10.3 0.2 slice_reduce_fusion
  10.9 2.4 scatter_custom_fusion
  13.4 1.5 fusion
  14.9 1.5 fusion.2
  16.5 6.0 %gather_fusion = bf16[1024,2048]{1,0:T(8,128)(2,1)} fusion(bf16[256,2048]{1,0:T(8,128)(2,1)S(1)} %fusion.2, s32[1024]{0:T(1024)S(1)} %fusion.23), kind=kCustom, calls=%fused_computation | custom fusion | bytes 8392704 | tf_op jit(solution)/shard_map/gather | solution.py:73
  22.5 3.8 %scatter_custom_fusion.1 = bf16[1024]{0:T(1024)(128)(2,1)S(1)} fusion(s32[512]{0:T(512)S(1)} %bitcast.38, bf16[512]{0:T(512)(128)(2,1)S(1)} %broadcast.155, bf16[]{:T(256)} %constant.70.clone.1), kind=kCustom, calls=%fused_computation.59 | custom fusion | bytes 2050 | tf_op jit(solution)/shard_map/scatter | solution.py:72
  26.3 4.5 %broadcast_multiply_fusion = bf16[8,128,2048]{2,1,0:T(8,128)(2,1)} fusion(bf16[8,128,2048]{2,1,0:T(8,128)(2,1)} %bitcast.34, bf16[8,128]{1,0:T(8,128)(2,1)S(1)} %bitcast.36), kind=kLoop, calls=%fused_computation.18 | loop fusion | flops 2097152 | bytes 8390656 | tf_op jit(solution)/shard_map/mul | solution.py:73
  30.7 7.3 %all-to-all-start = ((bf16[8,128,2048]{2,1,0:T(8,128)(2,1)}), bf16[8,128,2048]{2,1,0:T(8,128)(2,1)}, u32[]{:S(2)}, u32[]{:S(2)}) async-start(bf16[8,128,2048]{2,1,0:T(8,128)(2,1)} %broadcast_multiply_fusion), calls=%async_computation | async-start | bytes 8388608 | tf_op jit(solution)/shard_map/all_to_all | solution.py:74
  38.1 0.7 all-gather.2.cloned.1.call-update
  38.8 92.6 %all-to-all-done = bf16[8,128,2048]{2,1,0:T(8,128)(2,1)} async-done(((bf16[8,128,2048]{2,1,0:T(8,128)(2,1)}), bf16[8,128,2048]{2,1,0:T(8,128)(2,1)}, u32[]{:S(2)}, u32[]{:S(2)}) %all-to-all-start) | async-done | bytes 4194336 | tf_op jit(solution)/shard_map/all_to_all | solution.py:74
  131.3 6.6 %fusion.4 = f32[1024,512]{1,0:T(8,128)} fusion(bf16[1024,2048]{1,0:T(8,128)(2,1)} %bitcast.9, bf16[1,2048,512]{2,1,0:T(8,128)(2,1)} %param.24), kind=kOutput, calls=%fused_computation.13 | convolution fusion | flops 2147483648 | bytes 8388608 | tf_op jit(solution)/shard_map/dot_general | solution.py:77
  137.9 10.1 %convolution_convert_fusion = bf16[1024,2048]{1,0:T(8,128)(2,1)} fusion(bf16[1,512,2048]{2,1,0:T(8,128)(2,1)S(1)} %copy-done, f32[1024,512]{1,0:T(8,128)} %fusion.4, bf16[1024,2048]{1,0:T(8,128)(2,1)} %bitcast.9, bf16[1,2048,512]{2,1,0:T(8,128)(2,1)} %param.23), kind=kOutput, calls=%fused_computation.5 | convolution fusion | flops 4300210176 | bytes 14680064 | tf_op jit(solution)/shard_map/dot_general | solution.py:79
  148.0 4.7 %all-to-all-start.1 = ((bf16[8,128,2048]{2,1,0:T(8,128)(2,1)}), bf16[8,128,2048]{2,1,0:T(8,128)(2,1)}, u32[]{:S(2)}, u32[]{:S(2)}) async-start(bf16[8,128,2048]{2,1,0:T(8,128)(2,1)} %bitcast.35), calls=%async_computation.1 | async-start | bytes 8388608 | tf_op jit(solution)/shard_map/all_to_all | solution.py:83
  152.7 1.2 multiply_convert_fusion.2
  153.9 1.5 collective-permute-start
  155.7 0.3 collective-permute-done
  156.0 6.0 %convolution_convert_fusion.1 = bf16[128,2048]{1,0:T(8,128)(2,1)} fusion(bf16[2048,2048]{1,0:T(8,128)(2,1)} %all-gather.2.cloned.1.call-done, bf16[128,2048]{1,0:T(8,128)(2,1)S(1)} %multiply_convert_fusion.2, bf16[128,2048]{1,0:T(8,128)(2,1)} %param.13, bf16[2,2048]{1,0:T(2,128)(2,1)S(1)} %collective-permute-done, f32[2048]{0:T(1024)S(1)} %bitcast.41, ...), kind=kOutput, calls=%fused_computation.8 | convolution fusion | flops 1078984704 | bytes 9994496 | tf_op jit(solution)/shard_map/dot_general | solution.py:49
  162.1 83.2 %all-to-all-done.1 = bf16[8,128,2048]{2,1,0:T(8,128)(2,1)} async-done(((bf16[8,128,2048]{2,1,0:T(8,128)(2,1)}), bf16[8,128,2048]{2,1,0:T(8,128)(2,1)}, u32[]{:S(2)}, u32[]{:S(2)}) %all-to-all-start.1) | async-done | bytes 4194336 | tf_op jit(solution)/shard_map/all_to_all | solution.py:83
  245.2 8.0 %gather_fusion.1 = bf16[512,2048]{1,0:T(8,128)(2,1)} fusion(bf16[1024,2048]{1,0:T(8,128)(2,1)} %bitcast.14, s32[1024]{0:T(1024)S(1)} %pad_clamp_fusion), kind=kCustom, calls=%fused_computation.1 | custom fusion | bytes 4196352 | tf_op jit(solution)/shard_map/gather | solution.py:84
  253.2 5.4 %reshape.132 = f32[256,2,2048]{2,1,0:T(2,128)} reshape(bf16[512,2048]{1,0:T(8,128)(2,1)} %gather_fusion.1) | data formatting | bytes 6291456 | tf_op jit(solution)/shard_map/convert_element_type | solution.py:89
  258.7 9.9 %multiply_reduce_fusion = bf16[256,2048]{1,0:T(8,128)(2,1)} fusion(f32[256,2,2048]{2,1,0:T(2,128)} %reshape.132, f32[256,2]{1,0:T(8,128)S(1)} %copy.19), kind=kLoop, calls=%fused_computation.4 | loop fusion | flops 1572864 | bytes 5244928 | tf_op jit(solution)/shard_map/reduce_sum | solution.py:89
  (33 shorter events, 1.0 us)
Async XLA Ops:
  7.2 130.7 %copy-start = (bf16[1,512,2048]{2,1,0:T(8,128)(2,1)S(1)}, bf16[1,512,2048]{2,1,0:T(8,128)(2,1)}, u32[]{:S(2)}) copy-start(bf16[1,512,2048]{2,1,0:T(8,128)(2,1)} %param.25) | copy-start | bytes 6291460
  30.7 100.6 %all-to-all-start = ((bf16[8,128,2048]{2,1,0:T(8,128)(2,1)}), bf16[8,128,2048]{2,1,0:T(8,128)(2,1)}, u32[]{:S(2)}, u32[]{:S(2)}) async-start(bf16[8,128,2048]{2,1,0:T(8,128)(2,1)} %broadcast_multiply_fusion), calls=%async_computation | async-start | bytes 8388608 | tf_op jit(solution)/shard_map/all_to_all | solution.py:74
  38.0 118.0 %all-gather.2.cloned.1.call-start = ((), (), s32[]{:S(2)}) async-start(), calls=%async_computation.2 | async-start | bytes 10485760 | tf_op jit(solution)/shard_map/all_gather | solution.py:51
  148.0 4.8 %copy-start.1 = (bf16[128,2048]{1,0:T(8,128)(2,1)S(1)}, bf16[128,2048]{1,0:T(8,128)(2,1)}, u32[]{:S(2)}) copy-start(bf16[128,2048]{1,0:T(8,128)(2,1)} %param.15) | copy-start | bytes 1572868
  148.0 7.5 %copy-start.3 = (f32[256,2]{0,1:T(2,128)S(1)}, f32[256,2]{0,1:T(2,128)}, u32[]{:S(2)}) copy-start(f32[256,2]{0,1:T(2,128)} %param.21) | copy-start | bytes 6148
  148.0 7.5 %copy-start.4 = (f32[256]{0:T(256)S(1)}, f32[256]{0:T(256)}, u32[]{:S(2)}) copy-start(f32[256]{0:T(256)} %param.22) | copy-start | bytes 3076
  148.0 7.5 %copy-start.2 = (f32[3,2048]{1,0:T(4,128)S(1)}, f32[3,2048]{1,0:T(4,128)}, u32[]{:S(2)}) copy-start(f32[3,2048]{1,0:T(4,128)} %param.16) | copy-start | bytes 73732
  148.0 97.2 %all-to-all-start.1 = ((bf16[8,128,2048]{2,1,0:T(8,128)(2,1)}), bf16[8,128,2048]{2,1,0:T(8,128)(2,1)}, u32[]{:S(2)}, u32[]{:S(2)}) async-start(bf16[8,128,2048]{2,1,0:T(8,128)(2,1)} %bitcast.35), calls=%async_computation.1 | async-start | bytes 8388608 | tf_op jit(solution)/shard_map/all_to_all | solution.py:83
  153.9 2.1 collective-permute-start
Sparse Core Ops, SparseCore 0:
  40.4 59.6 all-gather.1
where the time goes:
time: 280 us; the launch traced here: 275 us
  waiting for transfers between devices  177 us (63%)
  local copies, waits for them, and re-layouts  27.6 us (10%)
  matrix products  22.6 us (8%)
  other arithmetic  20.6 us (7%)
  between operations  14.2 us (5%)
  starting transfers between devices  13.5 us (5%)
    all_to_all x1, waiting for transfers between devices, local(): lax.all_to_all(outgoing, 'ep', split_axis=0, concat_axis=0, tiled=True)  92.6 us
    all_to_all x1, waiting for transfers between devices, local(): lax.all_to_all(results, 'ep', split_axis=0, concat_axis=0, tiled=True)  83.2 us
    dot_general x1, matrix products, local(): jnp.dot(hidden, down_weight[0], preferred_element_type=jnp.float32)  10.1 us
    reduce_sum x1, other arithmetic, local(): jnp.sum(picked.astype(jnp.float32) * route_weight[:, :, None], axis=1)  9.86 us
    gather x1, local copies, waits for them, and re-layouts, local(): returned.reshape(experts * capacity, width)[target]  8 us
    all_to_all x1, starting transfers between devices, local(): lax.all_to_all(outgoing, 'ep', split_axis=0, concat_axis=0, tiled=True)  7.28 us
    dot_general x1, matrix products, local(): upper = jnp.dot(rows, up_weight[0], preferred_element_type=jnp.float32)  6.56 us
    gather x1, local copies, waits for them, and re-layouts, local(): normed[owner] * filled[:, None]  6.02 us
  transfers between devices with their start and end apart: 4, of which 3 were waited for; matrix products, arithmetic and copies ran while one was open for 9% of the time, Pallas kernels for 0%

commit v1 on v0

v1 whole, which is shorter than its diff:
```python
import functools
import math

import jax
import jax.numpy as jnp
from jax import lax
from jax.experimental import pallas as pl
from jax.experimental.pallas import tpu as pltpu
from jax.sharding import PartitionSpec as P

SEQS = 1

norm_eps = 1e-05

F32 = jnp.float32
BF16 = jnp.bfloat16
LANES = 128
VMEM_BYTES = 40 * 1024 * 1024


def plane_shape(ep):
    across = math.isqrt(ep // 2)
    if across < 1 or 2 * across * across != ep:
        across = 1
    return ep // across, across


def pack_weights(gate, up, down, part, parts):
    width, units = gate.shape
    share = units // parts
    half = width // 2
    step = 2 * share

    def body(_, gate_ref, up_ref, down_ref, low_ref, high_ref, out_ref):
        low_ref[:, :share] = gate_ref[:half, :]
        low_ref[:, share:] = up_ref[:half, :]
        high_ref[:, :share] = gate_ref[half:, :]
        high_ref[:, share:] = up_ref[half:, :]
        for i in range(width // step):
            out_ref[i * share : (i + 1) * share, :] = down_ref[:, i * step : (i + 1) * step]

    piece = jax.ShapeDtypeStruct((half, step), BF16)
    return pl.pallas_call(
        body,
        grid_spec=pltpu.PrefetchScalarGridSpec(
            num_scalar_prefetch=1,
            grid=(1,),
            in_specs=[
                pl.BlockSpec((width, share), lambda i, p: (0, p[0])),
                pl.BlockSpec((width, share), lambda i, p: (0, p[0])),
                pl.BlockSpec((share, width), lambda i, p: (p[0], 0)),
            ],
            out_specs=[pl.BlockSpec((half, step), lambda i, p: (0, 0))] * 3,
        ),
        out_shape=[piece] * 3,
        compiler_params=pltpu.CompilerParams(vmem_limit_bytes=16 * 1024 * 1024),
        name="pack_weights",
    )(part, gate, up, down)


def ffn(slots, scalars, experts, meta, gain, own, pieces):
    arrays = [array for slot in slots for array in slot]
    tokens, width = arrays[0].shape
    gate, up, down = own
    units = gate.shape[1]
    others = len(pieces)
    flat = [part for shares in pieces for share in shares for part in share]
    column = 2 * LANES

    def body(scalar_ref, expert_ref, *refs):
        in_refs = refs[: len(arrays)]
        meta_ref, gain_ref, gate_ref, up_ref, down_ref = refs[len(arrays) : len(arrays) + 5]
        rest = refs[len(arrays) + 5 :]
        piece_refs = rest[: len(flat)]
        out_refs = rest[len(flat) : len(flat) + len(slots)]
        normed_ref, hidden_ref = rest[len(flat) + len(slots) :]

        def block(x_ref, origin, out_ref):
            x = x_ref[...].astype(F32)
            scale = lax.rsqrt(jnp.mean(x * x, axis=-1, keepdims=True) + norm_eps)
            normed_ref[...] = (x * scale * gain_ref[...]).astype(BF16)
            info = meta_ref[origin]
            rows = []
            for j in range(others + 1):
                expert = expert_ref[j].astype(F32)
                rows.append(
                    jnp.where(info[0:1] == expert, info[2:3], 0.0)
                    + jnp.where(info[1:2] == expert, info[3:4], 0.0)
                )
            rows.append(jnp.zeros((LANES - others - 1, tokens), F32))
            weights = jnp.concatenate(rows, axis=0).T
            normed = normed_ref[...]
            first = jnp.dot(normed, gate_ref[...], preferred_element_type=F32)
            second = jnp.dot(normed, up_ref[...], preferred_element_type=F32)
            hidden_ref[:, :units] = (jax.nn.silu(first) * second * weights[:, 0:1]).astype(BF16)
            at = units
            k = 0
            half = width // 2
            for j in range(others):
                for low, high, _ in pieces[j]:
                    share = low.shape[1] // 2
                    both = jnp.dot(
                        normed_ref[:, :half], piece_refs[k][...], preferred_element_type=F32
                    ) + jnp.dot(
                        normed_ref[:, half:], piece_refs[k + 1][...], preferred_element_type=F32
                    )
                    value = jax.nn.silu(both[:, :share]) * both[:, share:]
                    hidden_ref[:, at : at + share] = (value * weights[:, j + 1 : j + 2]).astype(BF16)
                    at += share
                    k += 3
            for i in range(width // column):
                total = jnp.dot(
                    hidden_ref[:, :units],
                    down_ref[:, i * column : (i + 1) * column],
                    preferred_element_type=F32,
                )
                k = 0
                at = units
                for j in range(others):
                    stack = []
                    for low, high, _ in pieces[j]:
                        share = low.shape[1] // 2
                        step = 2 * share
                        if step == column:
                            stack.append(piece_refs[k + 2][i * share : (i + 1) * share, :])
                        k += 3
                    total += jnp.dot(
                        hidden_ref[:, at : at + units],
                        jnp.concatenate(stack, axis=0),
                        preferred_element_type=F32,
                    )
                    at += units
                out_ref[:, i * column : (i + 1) * column] = total.astype(BF16)

        at = 0
        for out_ref, slot in zip(out_refs, slots):
            for _ in slot:

                @pl.when(scalar_ref[2 * at] == 1)
                def _(x_ref=in_refs[at], at=at, out_ref=out_ref):
                    block(x_ref, scalar_ref[2 * at + 1], out_ref)

                at += 1

    inputs = [scalars, experts, *arrays, meta, gain, gate, up, down, *flat]
    vmem = pl.BlockSpec(memory_space=pltpu.VMEM)
    smem = pl.BlockSpec(memory_space=pltpu.SMEM)
    weight_count = (others + 1) * 3 * width * units
    return pl.pallas_call(
        body,
        in_specs=[smem, smem] + [vmem] * (len(inputs) - 2),
        out_specs=[vmem] * len(slots),
        out_shape=[jax.ShapeDtypeStruct((tokens, width), BF16)] * len(slots),
        scratch_shapes=[
            pltpu.VMEM((tokens, width), BF16),
            pltpu.VMEM((tokens, (others + 1) * units), BF16),
        ],
        compiler_params=pltpu.CompilerParams(vmem_limit_bytes=VMEM_BYTES),
        cost_estimate=pl.CostEstimate(
            flops=2 * tokens * weight_count * len(slots),
            bytes_accessed=2 * weight_count + 4 * tokens * width * len(slots),
            transcendentals=tokens * units * (others + 1) * len(slots),
        ),
        name="ffn",
    )(*inputs)


def mixer(out_gate, in_gate, values, conv_taps, out_weight):
    rows_mix, width = out_gate.shape
    extent = conv_taps.shape[0] - 1
    tp = lax.axis_size("tp")
    devices = lax.axis_size("ep") * tp
    gated = (in_gate.astype(F32) * values.astype(F32)).astype(BF16)
    before = lax.ppermute(
        gated[rows_mix - extent :], ("ep", "tp"), [(i, i + 1) for i in range(devices - 1)]
    )
    extended = jnp.concatenate([before, gated], axis=0)
    seq_len = devices * rows_mix // SEQS
    position = lax.axis_index(("ep", "tp")) * rows_mix + jnp.arange(rows_mix, dtype=jnp.int32)
    offset = position % seq_len
    filtered = jnp.zeros((rows_mix, width), F32)
    for delays in range(extent + 1):
        lagged = extended[extent - delays : extent - delays + rows_mix].astype(F32)
        if delays > 0:
            lagged = jnp.where((offset >= delays)[:, None], lagged, 0.0)
        filtered = filtered + conv_taps[extent - delays] * lagged
    mixed = (out_gate.astype(F32) * filtered).astype(BF16)
    pieces = []
    for k in range(tp):
        there = mixed
        if k:
            there = lax.ppermute(mixed, "tp", [(i, (i + k) % tp) for i in range(tp)])
        product = jnp.dot(there, out_weight, preferred_element_type=F32).astype(BF16)
        if k:
            product = lax.ppermute(product, "tp", [((i + k) % tp, i) for i in range(tp)])
        pieces.append(product)
    me = lax.axis_index("tp")
    columns = out_weight.shape[1]
    result = jnp.zeros((rows_mix, tp * columns), BF16)
    for k, piece in enumerate(pieces):
        result = lax.dynamic_update_slice(result, piece, (0, (me + k) % tp * columns))
    return result


def local(
    out_gate,
    in_gate,
    values,
    conv_taps,
    out_weight,
    expert_input,
    norm_gain,
    expert_ids,
    route_logits,
    group_share,
    gate_weight,
    up_weight,
    down_weight,
):
    ep, tp = lax.axis_size("ep"), lax.axis_size("tp")
    planes, across = plane_shape(ep)
    me_ep, me_tp = lax.axis_index("ep"), lax.axis_index("tp")
    z, x = me_ep // across, me_ep % across
    units = gate_weight.shape[2]
    width = expert_input.shape[1]

    def along(value, pairs):
        whole = [(a * across + c, b * across + c) for a, b in pairs for c in range(across)]
        return lax.ppermute(value, "ep", whole)

    margin = route_logits[:, 0] - route_logits[:, 1]
    meta = jnp.stack(
        [
            expert_ids[:, 0].astype(F32),
            expert_ids[:, 1].astype(F32),
            group_share * jax.nn.sigmoid(margin),
            group_share * jax.nn.sigmoid(-margin),
        ]
    )
    meta = lax.all_gather(meta, "ep", axis=0)

    gate, up, down = gate_weight[0], up_weight[0], down_weight[0]
    parts = min(tp, units // LANES)
    others = []
    if across > 1:
        mine = pack_weights(gate, up, down, (me_tp % parts).reshape(1), parts)
        lanes = 2 if parts % 2 == 0 else 1
        for k in range(1, across):
            got = [
                lax.ppermute(
                    piece,
                    "ep",
                    [
                        (a * across + (c + k) % across, a * across + c)
                        for a in range(planes)
                        for c in range(across)
                    ],
                )
                for piece in mine
            ]
            shares = [got]
            for m in range(1, parts // lanes):
                pairs = [
                    (i, i // parts * parts + (i % parts + m * lanes) % parts) for i in range(tp)
                ]
                shares.append([lax.ppermute(piece, "tp", pairs) for piece in got])
            if lanes == 2:
                pairs = [(i, i ^ 1) for i in range(tp)]
                shares += [[lax.ppermute(piece, "tp", pairs) for piece in share] for share in shares]
            others.append(shares)
    experts = jnp.stack([z * across + (x + k) % across for k in range(across)]).astype(jnp.int32)

    gain = norm_gain.reshape(1, width)

    def run(slots):
        scalars = []
        for slot in slots:
            for _, away in slot:
                plane = z + away
                valid = (plane >= 0) & (plane < planes)
                origin = jnp.clip(plane, 0, planes - 1) * across + x
                scalars += [valid.astype(jnp.int32), origin.astype(jnp.int32)]
        return ffn(
            [[array for array, _ in slot] for slot in slots],
            jnp.stack(scalars),
            experts,
            meta,
            gain,
            (gate, up, down),
            others,
        )

    own = expert_input
    low = (planes + 1) // 2
    seen = {}
    for d in range(planes - 1, 2, -1):
        to_low = [(a, a - d) for a in range(d, planes)]
        to_high = [(a, a + d) for a in range(planes - d)]
        if d >= low:
            both = along(own, to_low + to_high)
            seen[d] = (both, both)
        else:
            seen[d] = (along(own, to_low), along(own, to_high))
    if planes > 1:
        seen[1] = (
            along(own, [(a, a - 1) for a in range(1, planes)]),
            along(own, [(a, a + 1) for a in range(planes - 1)]),
        )
    if planes > 2:
        seen[2] = (
            along(seen[1][0], [(a, a - 1) for a in range(1, planes - 1)]),
            along(seen[1][1], [(a, a + 1) for a in range(1, planes - 1)]),
        )

    partial = {}
    for d in range(planes - 1, 2, -1):
        if d >= low:
            partial[d] = run([[(seen[d][0], d), (seen[d][1], -d)]]) * 2
        else:
            partial[d] = run([[(seen[d][0], d)], [(seen[d][1], -d)]])
    near = [[(own, 0)]]
    if planes > 1:
        near += [[(seen[1][0], 1)], [(seen[1][1], -1)]]
    near = run(near)
    if planes > 1:
        partial[1] = near[1:]
    if planes > 2:
        if 2 >= low:
            partial[2] = run([[(seen[2][0], 2), (seen[2][1], -2)]]) * 2
        else:
            partial[2] = run([[(seen[2][0], 2)], [(seen[2][1], -2)]])

    def plus(a, b):
        return (a.astype(F32) + b.astype(F32)).astype(BF16)

    came = None
    for d in range(planes - 1, 0, -1):
        up_pairs = [(a, a + 1) for a in range(planes - d)]
        down_pairs = [(a, a - 1) for a in range(d, planes)]
        if d >= low:
            send = partial[d][0]
            if came is not None:
                send = plus(send, came[0])
            if {b for _, b in up_pairs} & {b for _, b in down_pairs}:
                came = (along(send, up_pairs), along(send, down_pairs))
            else:
                came = (along(send, up_pairs + down_pairs),) * 2
        else:
            send = partial[d]
            if came is not None:
                send = [plus(send[0], came[0]), plus(send[1], came[1])]
            came = (along(send[0], up_pairs), along(send[1], down_pairs))
    total = near[0].astype(F32)
    if came is not None:
        total = total + came[0].astype(F32) + came[1].astype(F32)
    expert_mix = total.astype(BF16)

    mixer_out = mixer(out_gate, in_gate, values, conv_taps, out_weight)
    return (mixer_out, expert_mix)


def solution(mesh):
    return jax.shard_map(
        local,
        mesh=mesh,
        in_specs=(
            P(("ep", "tp"), None),
            P(("ep", "tp"), None),
            P(("ep", "tp"), None),
            P(),
            P(None, "tp"),
            P(("ep", "tp"), None),
            P(),
            P(("ep", "tp"), None),
            P(("ep", "tp"), None),
            P(("ep", "tp")),
            P("ep", None, None),
            P("ep", None, None),
            P("ep", None, None),
        ),
        out_specs=(P(("ep", "tp"), None), P(("ep", "tp"), None)),
        check_vma=False,
    )
```

time: 280 us -> 233 us (0.83); the launches traced: 275 us -> 231 us
  waiting for transfers between devices: 177 us -> 75.7 us
  blocking collectives: 0 us -> 51.4 us
  starting transfers between devices: 13.5 us -> 42.2 us
  Pallas kernels: 0 us -> 26.5 us
  matrix products: 22.6 us -> 1.81 us
  other arithmetic: 20.6 us -> 7.53 us
  between operations: 14.2 us -> 1.31 us
    all_to_all x2 -> x0, waiting for transfers between devices: 176 us -> none  [the longest x1 92.6 us: local(): lax.all_to_all(outgoing, 'ep', split_axis=0, concat_axis=0, tiled=True)]
    ppermute x1 -> x29, waiting for transfers between devices: 0.34 us -> 75.7 us  [the longest x10 39.8 us: along(): return lax.ppermute(value, 'ep', whole)]
    all_gather x0 -> x1, blocking collectives: none -> 51.4 us  [local(): meta = lax.all_gather(meta, 'ep', axis=0)]
    ppermute x1 -> x29, starting transfers between devices: 1.47 us -> 42.2 us  [the longest x10 27.5 us: along(): return lax.ppermute(value, 'ep', whole)]
    pallas_call x0 -> x4, Pallas kernels: none -> 26.5 us  [the longest x3 26.1 us: ffn(): pl.pallas_call(body, in_specs=[smem, smem] + [vmem] * (len(inputs) - 2),...]
    unnamed x11 -> x82, local copies, waits for them, and re-layouts: 0.98 us -> 24 us
    dot_general x3 -> x4, matrix products: 22.6 us -> 1.81 us  [mixer(): jnp.dot(there, out_weight, preferred_element_type=F32).astype(BF16)]
    gather x2 -> x0, local copies, waits for them, and re-layouts: 14 us -> none  [the longest x1 8 us: local(): returned.reshape(experts * capacity, width)[target]]
  transfers between devices with their start and end apart: 4 -> 29, of which waited for: 3 -> 14; matrix products, arithmetic and copies ran while one was open for 9% -> 4% of each run, Pallas kernels for 0% -> 11%
where the time goes in v1:
time: 233 us; the launch traced here: 231 us
  waiting for transfers between devices  75.7 us (32%)
  blocking collectives  51.4 us (22%)
  starting transfers between devices  42.2 us (18%)
  Pallas kernels  26.5 us (11%)
  local copies, waits for them, and re-layouts  25 us (11%)
  other arithmetic  7.53 us (3%)
    all_gather x1, blocking collectives, local(): meta = lax.all_gather(meta, 'ep', axis=0)  51.4 us
    ppermute x10, waiting for transfers between devices, along(): return lax.ppermute(value, 'ep', whole)  39.8 us
    ppermute x3, waiting for transfers between devices, local(): lax.ppermute(piece, 'ep', [(a * across + (c + k) % across, a * across + c...  28.4 us
    ppermute x10, starting transfers between devices, along(): return lax.ppermute(value, 'ep', whole)  27.5 us
    pallas_call x3, Pallas kernels, ffn(): pl.pallas_call(body, in_specs=[smem, smem] + [vmem] * (len(inputs) - 2),...  26.1 us
    unnamed x82, local copies, waits for them, and re-layouts  24 us
    ppermute x3, waiting for transfers between devices, mixer(): lax.ppermute(product, 'tp', [((i + k) % tp, i) for i in range(tp)])  6.23 us
    ppermute x3, starting transfers between devices, local(): shares.append([lax.ppermute(piece, 'tp', pairs) for piece in got])  5.86 us
  transfers between devices with their start and end apart: 29, of which 14 were waited for; matrix products, arithmetic and copies ran while one was open for 4% of the time, Pallas kernels for 11%

profile of v1, /device:TPU:0, one launch (start us, length us, event | category | flops | bytes accessed | tf_op | source)
XLA Modules:
  0.0 231.4 jit_solution(17608623941446813783)
XLA Ops:
  6.0 3.0 %collective-permute-start.9 = (bf16[1024,256]{1,0:T(8,128)(2,1)S(1)}, bf16[1024,256]{1,0:T(8,128)(2,1)S(1)}, u32[]{:S(2)}, u32[]{:S(2)}) collective-permute-start(bf16[1024,256]{1,0:T(8,128)(2,1)S(1)} %get-tuple-element.8), channel_id=1, source_target_pairs={{4,0},{0,4},{12,8},{8,12},{20,16},{16,20},{28,24},{24,28},{5,1},{1... | collective-permute-start | bytes 1572872 | tf_op jit(solution)/shard_map/ppermute | solution.py:250
  11.1 10.7 %collective-permute-done.9.refs_8_.refs_7_ = bf16[1024,256]{1,0:T(8,128)(2,1)S(1)} collective-permute-done((bf16[1024,256]{1,0:T(8,128)(2,1)S(1)}, bf16[1024,256]{1,0:T(8,128)(2,1)S(1)}, u32[]{:S(2)}, u32[]{:S(2)}) %collective-permute-start.9) | collective-permute-done | bytes 524320 | tf_op jit(solution)/shard_map/ppermute | solution.py:250
  21.8 2.0 collective-permute-start.12
  23.9 9.3 %collective-permute-done.10.refs_9_.refs_8_ = bf16[1024,256]{1,0:T(8,128)(2,1)} collective-permute-done((bf16[1024,256]{1,0:T(8,128)(2,1)S(1)}, bf16[1024,256]{1,0:T(8,128)(2,1)}, u32[]{:S(2)}, u32[]{:S(2)}) %collective-permute-start.10) | collective-permute-done | bytes 524320 | tf_op jit(solution)/shard_map/ppermute | solution.py:250
  33.2 2.0 collective-permute-start.13
  35.2 8.3 %collective-permute-done.11.refs_10_.refs_9_ = bf16[1024,256]{1,0:T(8,128)(2,1)} collective-permute-done((bf16[1024,256]{1,0:T(8,128)(2,1)S(1)}, bf16[1024,256]{1,0:T(8,128)(2,1)}, u32[]{:S(2)}, u32[]{:S(2)}) %collective-permute-start.11) | collective-permute-done | bytes 524320 | tf_op jit(solution)/shard_map/ppermute | solution.py:250
  47.6 5.5 %collective-permute-start.8 = (bf16[256,2048]{1,0:T(8,128)(2,1)}, bf16[256,2048]{1,0:T(8,128)(2,1)}, u32[]{:S(2)}, u32[]{:S(2)}) collective-permute-start(bf16[256,2048]{1,0:T(8,128)(2,1)} %refs_0_.1), channel_id=1, source_target_pairs={{0,8},{4,12},{8,16},{12,20},{16,24},{20,28},{1,9},{5,13},{9,17},{1... | collective-permute-start | bytes 3145736 | tf_op jit(solution)/shard_map/ppermute | solution.py:229
  53.1 3.4 %collective-permute-start.23 = (bf16[256,2048]{1,0:T(8,128)(2,1)}, bf16[256,2048]{1,0:T(8,128)(2,1)S(1)}, u32[]{:S(2)}, u32[]{:S(2)}) collective-permute-start(bf16[256,2048]{1,0:T(8,128)(2,1)} %refs_0_.1), channel_id=1, source_target_pairs={{24,0},{28,4},{0,24},{4,28},{25,1},{29,5},{1,25},{5,29},{26,2},{30... | collective-permute-start | bytes 3145736 | tf_op jit(solution)/shard_map/ppermute | solution.py:229
  60.5 12.6 %collective-permute-done.7.refs_1_ = bf16[256,2048]{1,0:T(8,128)(2,1)} collective-permute-done((bf16[256,2048]{1,0:T(8,128)(2,1)}, bf16[256,2048]{1,0:T(8,128)(2,1)}, u32[]{:S(2)}, u32[]{:S(2)}) %collective-permute-start.7) | collective-permute-done | bytes 1048608 | tf_op jit(solution)/shard_map/ppermute | solution.py:229
  73.1 51.4 %all-gather.1.refs_3_.refs_2_ = f32[8,4,256]{2,1,0:T(4,128)S(1)} all-gather(f32[1,4,256]{2,1,0:T(4,128)S(1)} %maximum_bitcast_fusion), channel_id=2, replica_groups=mesh['ep'=8,'tp'=4] {'ep'}, dimensions={0}, use_global_device_ids=true | all-gather | bytes 36864 | tf_op jit(solution)/shard_map/all_gather | solution.py:240
  128.9 2.0 copy-done.2
  137.7 7.1 %ffn.5 = bf16[256,2048]{1,0:T(8,128)(2,1)} custom-call(s32[4]{0:T(128)S(1)} %pad_add_fusion.2.scalar_ref, s32[2]{0:T(128)S(1)} %pad_add_fusion.expert_ref, bf16[256,2048]{1,0:T(8,128)(2,1)S(1)} %collective-permute-done.23.refs_0_.refs_1_, bf16[256,2048]{1,0:T(8,128)(2,1)S(1)} %collective-permute-done.23.refs_0_.refs_1_, ...), custom_call_target="tpu_custom_call" | custom-call | flops 3221225472 | bytes 14680064 | tf_op jit(solution)/shard_map/ffn/pallas_call | solution.py:149
  144.8 3.4 %collective-permute-start.24 = (bf16[256,2048]{1,0:T(8,128)(2,1)}, bf16[256,2048]{1,0:T(8,128)(2,1)}, u32[]{:S(2)}, u32[]{:S(2)}) collective-permute-start(bf16[256,2048]{1,0:T(8,128)(2,1)} %ffn.5), channel_id=1, source_target_pairs={{0,8},{4,12},{24,16},{28,20},{1,9},{5,13},{25,17},{29,21},{2,10},{... | collective-permute-start | bytes 3145736 | tf_op jit(solution)/shard_map/ppermute | solution.py:229
  148.5 2.4 %multiply_convert_fusion = bf16[128,2048]{1,0:T(8,128)(2,1)S(1)} fusion(bf16[128,2048]{1,0:T(8,128)(2,1)} %multiply_convert_fusion.1, bf16[128,2048]{1,0:T(8,128)(2,1)} %param.13, bf16[2,2048]{1,0:T(2,128)(2,1)S(1)} %collective-permute-done, f32[2048]{0:T(1024)S(1)} %bitcast.58, f32[2048]{0:T(1024)S(1)} %bitcast.59, f32[2048]{0:T(1024)S(1)} %bitcast.57, ...), kind=kLoop, calls=%fused_computation.9 | loop fusion | flops 4980736 | bytes 1605888 | tf_op jit(solution)/shard_map/convert_element_type | solution.py:187
  151.5 2.4 %collective-permute-done.21.refs_0_ = bf16[256,2048]{1,0:T(8,128)(2,1)} collective-permute-done((bf16[256,2048]{1,0:T(8,128)(2,1)}, bf16[256,2048]{1,0:T(8,128)(2,1)}, u32[]{:S(2)}, u32[]{:S(2)}) %collective-permute-start.21) | collective-permute-done | bytes 1048608 | tf_op jit(solution)/shard_map/ppermute | solution.py:229
  163.5 6.9 %ffn.4 = bf16[256,2048]{1,0:T(8,128)(2,1)S(1)} custom-call(s32[4]{0:T(128)S(1)} %pad_add_fusion.1.scalar_ref, s32[2]{0:T(128)S(1)} %pad_add_fusion.expert_ref, bf16[256,2048]{1,0:T(8,128)(2,1)} %collective-permute-done.21.refs_0_, bf16[256,2048]{1,0:T(8,128)(2,1)} %collective-permute-done.22.refs_1_, f32[8,4,256]{2,1,0:T(4,128)S(1)} %all-gather.1.refs_3_.refs_2_, ...), custom_call_target="tpu_custom_call" | custom-call | flops 3221225472 | bytes 14680064 | tf_op jit(solution)/shard_map/ffn/pallas_call | solution.py:149
  172.3 4.6 %collective-permute-start.25 = (bf16[256,2048]{1,0:T(8,128)(2,1)S(1)}, bf16[256,2048]{1,0:T(8,128)(2,1)S(1)}, u32[]{:S(2)}, u32[]{:S(2)}) collective-permute-start(bf16[256,2048]{1,0:T(8,128)(2,1)S(1)} %add_convert_fusion.3), channel_id=1, source_target_pairs={{0,8},{4,12},{8,16},{12,20},{1,9},{5,13},{9,17},{13,21},{2,10},{6,... | collective-permute-start | bytes 3145736 | tf_op jit(solution)/shard_map/ppermute | solution.py:229
  178.2 12.2 %ffn.3 = (bf16[256,2048]{1,0:T(8,128)(2,1)S(1)}, bf16[256,2048]{1,0:T(8,128)(2,1)S(1)}, bf16[256,2048]{1,0:T(8,128)(2,1)S(1)}) custom-call(s32[6]{0:T(128)S(1)} %stack.101.scalar_ref, s32[2]{0:T(128)S(1)} %pad_add_fusion.expert_ref, bf16[256,2048]{1,0:T(8,128)(2,1)} %refs_0_.1, bf16[256,2048]{1,0:T(8,128)(2,1)} %collective-permute-done.7.refs_1_, ...), custom_call_target="tpu_custom_call" | custom-call | flops 9663676416 | bytes 18874368 | tf_op jit(solution)/shard_map/ffn/pallas_call | solution.py:149
  190.4 8.7 %collective-permute-done.25 = bf16[256,2048]{1,0:T(8,128)(2,1)S(1)} collective-permute-done((bf16[256,2048]{1,0:T(8,128)(2,1)S(1)}, bf16[256,2048]{1,0:T(8,128)(2,1)S(1)}, u32[]{:S(2)}, u32[]{:S(2)}) %collective-permute-start.25) | collective-permute-done | bytes 1048608 | tf_op jit(solution)/shard_map/ppermute | solution.py:229
  199.5 4.5 %collective-permute-start.26 = (bf16[256,2048]{1,0:T(8,128)(2,1)S(1)}, bf16[256,2048]{1,0:T(8,128)(2,1)S(1)}, u32[]{:S(2)}, u32[]{:S(2)}) collective-permute-start(bf16[256,2048]{1,0:T(8,128)(2,1)S(1)} %add_convert_fusion.2), channel_id=1, source_target_pairs={{0,8},{4,12},{8,16},{12,20},{16,24},{20,28},{1,9},{5,13},{9,17},{1... | collective-permute-start | bytes 3145736 | tf_op jit(solution)/shard_map/ppermute | solution.py:229
  207.7 2.0 collective-permute-done.2
  209.7 3.4 %collective-permute-done.4 = bf16[128,512]{1,0:T(8,128)(2,1)S(1)} collective-permute-done((bf16[128,512]{1,0:T(8,128)(2,1)S(1)}, bf16[128,512]{1,0:T(8,128)(2,1)S(1)}, u32[]{:S(2)}, u32[]{:S(2)}) %collective-permute-start.4) | collective-permute-done | bytes 131104 | tf_op jit(solution)/shard_map/ppermute | solution.py:195
  214.0 11.2 %collective-permute-done.26 = bf16[256,2048]{1,0:T(8,128)(2,1)S(1)} collective-permute-done((bf16[256,2048]{1,0:T(8,128)(2,1)S(1)}, bf16[256,2048]{1,0:T(8,128)(2,1)S(1)}, u32[]{:S(2)}, u32[]{:S(2)}) %collective-permute-start.26) | collective-permute-done | bytes 1048608 | tf_op jit(solution)/shard_map/ppermute | solution.py:229
  225.3 4.6 %collective-permute-done.28 = bf16[256,2048]{1,0:T(8,128)(2,1)S(1)} collective-permute-done((bf16[256,2048]{1,0:T(8,128)(2,1)S(1)}, bf16[256,2048]{1,0:T(8,128)(2,1)S(1)}, u32[]{:S(2)}, u32[]{:S(2)}) %collective-permute-start.28) | collective-permute-done | bytes 1048608 | tf_op jit(solution)/shard_map/ppermute | solution.py:229
  (147 shorter events, 46.6 us)
Async XLA Ops:
  6.0 15.8 %collective-permute-start.9 = (bf16[1024,256]{1,0:T(8,128)(2,1)S(1)}, bf16[1024,256]{1,0:T(8,128)(2,1)S(1)}, u32[]{:S(2)}, u32[]{:S(2)}) collective-permute-start(bf16[1024,256]{1,0:T(8,128)(2,1)S(1)} %get-tuple-element.8), channel_id=1, source_target_pairs={{4,0},{0,4},{12,8},{8,12},{20,16},{16,20},{28,24},{24,28},{5,1},{1... | collective-permute-start | bytes 1572872 | tf_op jit(solution)/shard_map/ppermute | solution.py:250
  9.1 24.1 %collective-permute-start.10 = (bf16[1024,256]{1,0:T(8,128)(2,1)S(1)}, bf16[1024,256]{1,0:T(8,128)(2,1)}, u32[]{:S(2)}, u32[]{:S(2)}) collective-permute-start(bf16[1024,256]{1,0:T(8,128)(2,1)S(1)} %get-tuple-element.9), channel_id=1, source_target_pairs={{4,0},{0,4},{12,8},{8,12},{20,16},{16,20},{28,24},{24,28},{5,1},{1... | collective-permute-start | bytes 1572872 | tf_op jit(solution)/shard_map/ppermute | solution.py:250
  9.1 34.4 %collective-permute-start.11 = (bf16[1024,256]{1,0:T(8,128)(2,1)S(1)}, bf16[1024,256]{1,0:T(8,128)(2,1)}, u32[]{:S(2)}, u32[]{:S(2)}) collective-permute-start(bf16[1024,256]{1,0:T(8,128)(2,1)S(1)} %get-tuple-element.10), channel_id=1, source_target_pairs={{4,0},{0,4},{12,8},{8,12},{20,16},{16,20},{28,24},{24,28},{5,1},{1... | collective-permute-start | bytes 1572872 | tf_op jit(solution)/shard_map/ppermute | solution.py:250
  21.8 25.7 %collective-permute-start.12 = (bf16[1024,256]{1,0:T(8,128)(2,1)S(1)}, bf16[1024,256]{1,0:T(8,128)(2,1)S(1)}, u32[]{:S(2)}, u32[]{:S(2)}) collective-permute-start(bf16[1024,256]{1,0:T(8,128)(2,1)S(1)} %collective-permute-done.9.refs_8_.refs_7_), channel_id=1, source_target_pairs={{0,2},{1,3},{2,0},{3,1},{4,6},{5,7},{6,4},{7,5},{8,10},{9,11},{10,... | collective-permute-start | bytes 1572872 | tf_op jit(solution)/shard_map/ppermute | solution.py:266
  33.2 19.9 %collective-permute-start.13 = (bf16[1024,256]{1,0:T(8,128)(2,1)}, bf16[1024,256]{1,0:T(8,128)(2,1)S(1)}, u32[]{:S(2)}, u32[]{:S(2)}) collective-permute-start(bf16[1024,256]{1,0:T(8,128)(2,1)} %collective-permute-done.10.refs_9_.refs_8_), channel_id=1, source_target_pairs={{0,2},{1,3},{2,0},{3,1},{4,6},{5,7},{6,4},{7,5},{8,10},{9,11},{10,... | collective-permute-start | bytes 1572872 | tf_op jit(solution)/shard_map/ppermute | solution.py:266
  43.6 13.3 %collective-permute-start.14 = (bf16[1024,256]{1,0:T(8,128)(2,1)}, bf16[1024,256]{1,0:T(8,128)(2,1)S(1)}, u32[]{:S(2)}, u32[]{:S(2)}) collective-permute-start(bf16[1024,256]{1,0:T(8,128)(2,1)} %collective-permute-done.11.refs_10_.refs_9_), channel_id=1, source_target_pairs={{0,2},{1,3},{2,0},{3,1},{4,6},{5,7},{6,4},{7,5},{8,10},{9,11},{10,... | collective-permute-start | bytes 1572872 | tf_op jit(solution)/shard_map/ppermute | solution.py:266
  45.3 11.5 %collective-permute-start.15 = (bf16[1024,256]{1,0:T(8,128)(2,1)S(1)}, bf16[1024,256]{1,0:T(8,128)(2,1)S(1)}, u32[]{:S(2)}, u32[]{:S(2)}) collective-permute-start(bf16[1024,256]{1,0:T(8,128)(2,1)S(1)} %collective-permute-done.9.refs_8_.refs_7_), channel_id=1, source_target_pairs={{0,1},{1,0},{2,3},{3,2},{4,5},{5,4},{6,7},{7,6},{8,9},{9,8},{10,11... | collective-permute-start | bytes 1572872 | tf_op jit(solution)/shard_map/ppermute | solution.py:269
  45.3 27.8 %collective-permute-start.7 = (bf16[256,2048]{1,0:T(8,128)(2,1)}, bf16[256,2048]{1,0:T(8,128)(2,1)}, u32[]{:S(2)}, u32[]{:S(2)}) collective-permute-start(bf16[256,2048]{1,0:T(8,128)(2,1)} %refs_0_.1), channel_id=1, source_target_pairs={{8,0},{12,4},{16,8},{20,12},{24,16},{28,20},{9,1},{13,5},{17,9},{2... | collective-permute-start | bytes 3145736 | tf_op jit(solution)/shard_map/ppermute | solution.py:229
  47.6 77.1 %collective-permute-start.8 = (bf16[256,2048]{1,0:T(8,128)(2,1)}, bf16[256,2048]{1,0:T(8,128)(2,1)}, u32[]{:S(2)}, u32[]{:S(2)}) collective-permute-start(bf16[256,2048]{1,0:T(8,128)(2,1)} %refs_0_.1), channel_id=1, source_target_pairs={{0,8},{4,12},{8,16},{12,20},{16,24},{20,28},{1,9},{5,13},{9,17},{1... | collective-permute-start | bytes 3145736 | tf_op jit(solution)/shard_map/ppermute | solution.py:229
  53.1 72.8 %collective-permute-start.23 = (bf16[256,2048]{1,0:T(8,128)(2,1)}, bf16[256,2048]{1,0:T(8,128)(2,1)S(1)}, u32[]{:S(2)}, u32[]{:S(2)}) collective-permute-start(bf16[256,2048]{1,0:T(8,128)(2,1)} %refs_0_.1), channel_id=1, source_target_pairs={{24,0},{28,4},{0,24},{4,28},{25,1},{29,5},{1,25},{5,29},{26,2},{30... | collective-permute-start | bytes 3145736 | tf_op jit(solution)/shard_map/ppermute | solution.py:229
  59.1 68.1 %collective-permute-start.18 = (bf16[1024,256]{1,0:T(8,128)(2,1)}, bf16[1024,256]{1,0:T(8,128)(2,1)S(1)}, u32[]{:S(2)}, u32[]{:S(2)}) collective-permute-start(bf16[1024,256]{1,0:T(8,128)(2,1)} %copy-done.11), channel_id=1, source_target_pairs={{0,1},{1,0},{2,3},{3,2},{4,5},{5,4},{6,7},{7,6},{8,9},{9,8},{10,11... | collective-permute-start | bytes 1572872 | tf_op jit(solution)/shard_map/ppermute | solution.py:269
  60.1 68.8 %collective-permute-start.19 = (bf16[1024,256]{1,0:T(8,128)(2,1)}, bf16[1024,256]{1,0:T(8,128)(2,1)S(1)}, u32[]{:S(2)}, u32[]{:S(2)}) collective-permute-start(bf16[1024,256]{1,0:T(8,128)(2,1)} %copy-done.14), channel_id=1, source_target_pairs={{0,1},{1,0},{2,3},{3,2},{4,5},{5,4},{6,7},{7,6},{8,9},{9,8},{10,11... | collective-permute-start | bytes 1572872 | tf_op jit(solution)/shard_map/ppermute | solution.py:269
  73.1 55.8 %collective-permute-start.20 = (bf16[1024,256]{1,0:T(8,128)(2,1)}, bf16[1024,256]{1,0:T(8,128)(2,1)S(1)}, u32[]{:S(2)}, u32[]{:S(2)}) collective-permute-start(bf16[1024,256]{1,0:T(8,128)(2,1)} %copy-done.17), channel_id=1, source_target_pairs={{0,1},{1,0},{2,3},{3,2},{4,5},{5,4},{6,7},{7,6},{8,9},{9,8},{10,11... | collective-permute-start | bytes 1572872 | tf_op jit(solution)/shard_map/ppermute | solution.py:269
  124.7 23.8 %collective-permute-start = (bf16[2,2048]{1,0:T(2,128)(2,1)S(1)}, bf16[2,2048]{1,0:T(2,128)(2,1)S(1)}, u32[]{:S(2)}, u32[]{:S(2)}) collective-permute-start(bf16[2,2048]{1,0:T(2,128)(2,1)S(1)} %slice.40), channel_id=1, source_target_pairs={{0,1},{1,2},{2,3},{3,4},{4,5},{5,6},{6,7},{7,8},{8,9},{9,10},{10,1... | collective-permute-start | bytes 24584 | tf_op jit(solution)/shard_map/ppermute | solution.py:174
  126.0 28.0 %collective-permute-start.21 = (bf16[256,2048]{1,0:T(8,128)(2,1)}, bf16[256,2048]{1,0:T(8,128)(2,1)}, u32[]{:S(2)}, u32[]{:S(2)}) collective-permute-start(bf16[256,2048]{1,0:T(8,128)(2,1)} %collective-permute-done.7.refs_1_), channel_id=1, source_target_pairs={{8,0},{12,4},{16,8},{20,12},{9,1},{13,5},{17,9},{21,13},{10,2},{14... | collective-permute-start | bytes 3145736 | tf_op jit(solution)/shard_map/ppermute | solution.py:229
  127.3 26.8 %collective-permute-start.22 = (bf16[256,2048]{1,0:T(8,128)(2,1)}, bf16[256,2048]{1,0:T(8,128)(2,1)}, u32[]{:S(2)}, u32[]{:S(2)}) collective-permute-start(bf16[256,2048]{1,0:T(8,128)(2,1)} %collective-permute-done.8.refs_2_), channel_id=1, source_target_pairs={{8,16},{12,20},{16,24},{20,28},{9,17},{13,21},{17,25},{21,29},{10,... | collective-permute-start | bytes 3145736 | tf_op jit(solution)/shard_map/ppermute | solution.py:229
  144.8 25.8 %collective-permute-start.24 = (bf16[256,2048]{1,0:T(8,128)(2,1)}, bf16[256,2048]{1,0:T(8,128)(2,1)}, u32[]{:S(2)}, u32[]{:S(2)}) collective-permute-start(bf16[256,2048]{1,0:T(8,128)(2,1)} %ffn.5), channel_id=1, source_target_pairs={{0,8},{4,12},{24,16},{28,20},{1,9},{5,13},{25,17},{29,21},{2,10},{... | collective-permute-start | bytes 3145736 | tf_op jit(solution)/shard_map/ppermute | solution.py:229
  150.8 54.8 %collective-permute-start.1 = (bf16[128,2048]{1,0:T(8,128)(2,1)S(1)}, bf16[128,2048]{1,0:T(8,128)(2,1)S(1)}, u32[]{:S(2)}, u32[]{:S(2)}) collective-permute-start(bf16[128,2048]{1,0:T(8,128)(2,1)S(1)} %multiply_convert_fusion), channel_id=1, source_target_pairs={{0,1},{1,2},{2,3},{3,0},{4,5},{5,6},{6,7},{7,4},{8,9},{9,10},{10,1... | collective-permute-start | bytes 1572872 | tf_op jit(solution)/shard_map/ppermute | solution.py:192
  151.2 55.0 %collective-permute-start.3 = (bf16[128,2048]{1,0:T(8,128)(2,1)S(1)}, bf16[128,2048]{1,0:T(8,128)(2,1)S(1)}, u32[]{:S(2)}, u32[]{:S(2)}) collective-permute-start(bf16[128,2048]{1,0:T(8,128)(2,1)S(1)} %multiply_convert_fusion), channel_id=1, source_target_pairs={{0,2},{1,3},{2,0},{3,1},{4,6},{5,7},{6,4},{7,5},{8,10},{9,11},{10,... | collective-permute-start | bytes 1572872 | tf_op jit(solution)/shard_map/ppermute | solution.py:192
  153.9 53.0 %collective-permute-start.5 = (bf16[128,2048]{1,0:T(8,128)(2,1)S(1)}, bf16[128,2048]{1,0:T(8,128)(2,1)S(1)}, u32[]{:S(2)}, u32[]{:S(2)}) collective-permute-start(bf16[128,2048]{1,0:T(8,128)(2,1)S(1)} %multiply_convert_fusion), channel_id=1, source_target_pairs={{0,3},{1,0},{2,1},{3,2},{4,7},{5,4},{6,5},{7,6},{8,11},{9,8},{10,9... | collective-permute-start | bytes 1572872 | tf_op jit(solution)/shard_map/ppermute | solution.py:192
  172.3 26.8 %collective-permute-start.25 = (bf16[256,2048]{1,0:T(8,128)(2,1)S(1)}, bf16[256,2048]{1,0:T(8,128)(2,1)S(1)}, u32[]{:S(2)}, u32[]{:S(2)}) collective-permute-start(bf16[256,2048]{1,0:T(8,128)(2,1)S(1)} %add_convert_fusion.3), channel_id=1, source_target_pairs={{0,8},{4,12},{8,16},{12,20},{1,9},{5,13},{9,17},{13,21},{2,10},{6,... | collective-permute-start | bytes 3145736 | tf_op jit(solution)/shard_map/ppermute | solution.py:229
  177.4 26.5 %collective-permute-start.27 = (bf16[256,2048]{1,0:T(8,128)(2,1)S(1)}, bf16[256,2048]{1,0:T(8,128)(2,1)S(1)}, u32[]{:S(2)}, u32[]{:S(2)}) collective-permute-start(bf16[256,2048]{1,0:T(8,128)(2,1)S(1)} %add_convert_fusion.3), channel_id=1, source_target_pairs={{16,8},{20,12},{24,16},{28,20},{17,9},{21,13},{25,17},{29,21},{18,... | collective-permute-start | bytes 3145736 | tf_op jit(solution)/shard_map/ppermute | solution.py:229
  199.5 25.8 %collective-permute-start.26 = (bf16[256,2048]{1,0:T(8,128)(2,1)S(1)}, bf16[256,2048]{1,0:T(8,128)(2,1)S(1)}, u32[]{:S(2)}, u32[]{:S(2)}) collective-permute-start(bf16[256,2048]{1,0:T(8,128)(2,1)S(1)} %add_convert_fusion.2), channel_id=1, source_target_pairs={{0,8},{4,12},{8,16},{12,20},{16,24},{20,28},{1,9},{5,13},{9,17},{1... | collective-permute-start | bytes 3145736 | tf_op jit(solution)/shard_map/ppermute | solution.py:229
  204.3 25.5 %collective-permute-start.28 = (bf16[256,2048]{1,0:T(8,128)(2,1)S(1)}, bf16[256,2048]{1,0:T(8,128)(2,1)S(1)}, u32[]{:S(2)}, u32[]{:S(2)}) collective-permute-start(bf16[256,2048]{1,0:T(8,128)(2,1)S(1)} %add_convert_fusion.1), channel_id=1, source_target_pairs={{8,0},{12,4},{16,8},{20,12},{24,16},{28,20},{9,1},{13,5},{17,9},{2... | collective-permute-start | bytes 3145736 | tf_op jit(solution)/shard_map/ppermute | solution.py:229
  (46 other events, 766.8 us)
